TPU v7x, 32 devices: a whole 2x2x4 slice. The times are simulated.
32 devices in a mesh: ep: 4 (over y, x), tp: 8 (over z, core).
Axes of the slice: x: 2, y: 2, z: 4, core: 2. Of those that a mesh axis runs over, the one named last changes fastest.
Arguments:
- tokens: bfloat16 [128, 2048], P(('ep', 'tp')), may hold values from -6 to 6
- lengths: int32 [128], P(('ep', 'tp')), may hold values from 64 to 1024
- cache_latent: bfloat16 [128, 1024, 512], P(('ep', 'tp')), may hold values from -6 to 6
- cache_rope_key: bfloat16 [128, 1024, 32], P(('ep', 'tp')), may hold values from -1000 to 1000
- route_ids: int32 [128, 4], P('ep'), may hold values from 0 to 31, all different within a row; in each aligned block of 32 rows (0 to 31, 32 to 63, ...) at most 8 rows name the same one
- route_weights: float32 [128, 4], P('ep'), may hold values from 0.2 to 2
- attn_gain: float32 [2048], replicated, may hold values from 0.1 to 1.9
- w_query_nope: bfloat16 [2048, 16, 64], P(None, 'tp'), may hold values from -0.125 to 0.125
- w_query_rope: bfloat16 [2048, 16, 32], P(None, 'tp'), may hold values from -0.125 to 0.125
- w_latent_down: bfloat16 [2048, 512], P(None, 'tp'), may hold values from -0.125 to 0.125
- w_key_rope: bfloat16 [2048, 32], replicated, may hold values from -0.125 to 0.125
- latent_gain: float32 [512], replicated, may hold values from 0.1 to 1.9
- w_key_up: bfloat16 [512, 16, 64], P(None, 'tp'), may hold values from -0.75 to 0.75
- w_value_up: bfloat16 [512, 16, 64], P(None, 'tp'), may hold values from -0.25 to 0.25
- w_attn_out: bfloat16 [16, 64, 2048], P('tp'), may hold values from -0.1875 to 0.1875
- ffn_gain: float32 [2048], replicated, may hold values from 0.1 to 1.9
- expert_gate: bfloat16 [32, 2048, 512], P(('ep', 'tp')), may hold values from -0.125 to 0.125
- expert_up: bfloat16 [32, 2048, 512], P(('ep', 'tp')), may hold values from -0.125 to 0.125
- expert_down: bfloat16 [32, 512, 2048], P(('ep', 'tp')), may hold values from -0.25 to 0.25
- shared_gate: bfloat16 [2048, 512], P(None, 'tp'), may hold values from -0.125 to 0.125
- shared_up: bfloat16 [2048, 512], P(None, 'tp'), may hold values from -0.125 to 0.125
- shared_down: bfloat16 [512, 2048], P('tp'), may hold values from -0.25 to 0.25
- dense_gate: bfloat16 [2048, 1024], P(None, 'tp'), may hold values from -0.125 to 0.125
- dense_up: bfloat16 [2048, 1024], P(None, 'tp'), may hold values from -0.125 to 0.125
- dense_down: bfloat16 [1024, 2048], P('tp'), may hold values from -0.1875 to 0.1875
- branch_gate: bfloat16 [2048], replicated, may hold values from -0.125 to 0.125
Outputs:
- mixed: bfloat16 [128, 2048], P(('ep', 'tp'))
- new_latent: bfloat16 [128, 512], P(('ep', 'tp'))
- new_rope_key: bfloat16 [128, 32], P(('ep', 'tp'))
Inputs may be any that keep to these rules, and one draw needn't show every extreme that they name: `route_ids`: in each aligned block of 32 rows, no expert is named by more than 8 of the block's rows, a bound that some block reaches. Each row names 4 different experts.
All inputs are finite; a program needn't handle non-finite values.
Results may differ from a plain program's by a relative error of at most 0.025.
Values may be sent and summed in bfloat16 or wider, within the bound.
A program may use at most 64 MiB of HBM per device.

v0:
```python
import jax
import jax.numpy as jnp
from jax import lax
from jax.sharding import PartitionSpec as P

epsilon = 1e-06
rope_base = 10000.0


def norm_rows(values, scales):
    values = values.astype(jnp.float32)
    factor = lax.rsqrt(jnp.mean(values * values, axis=-1, keepdims=True) + epsilon)
    return values * factor * scales


def rotate(values, positions):
    half_dim = values.shape[-1] // 2
    frequencies = rope_base ** (-jnp.arange(half_dim).astype(jnp.float32) / half_dim)
    angles = positions.astype(jnp.float32)[:, None] * frequencies[None, :]
    bcast_shape = (angles.shape[0],) + (1,) * (values.ndim - 2) + (half_dim,)
    cosine = jnp.cos(angles).reshape(bcast_shape)
    sine_val = jnp.sin(angles).reshape(bcast_shape)
    first_half = values[..., :half_dim].astype(jnp.float32)
    second_half = values[..., half_dim:].astype(jnp.float32)
    return jnp.concatenate(
        [
            first_half * cosine - second_half * sine_val,
            first_half * sine_val + second_half * cosine,
        ],
        axis=-1,
    )


def swiglu(inputs, gate_w, up_w):
    gate_val = jnp.dot(inputs, gate_w, preferred_element_type=jnp.float32)
    up_val = jnp.dot(inputs, up_w, preferred_element_type=jnp.float32)
    return (jax.nn.silu(gate_val) * up_val).astype(jnp.bfloat16)


def local(
    tokens,
    lengths,
    cache_latent,
    cache_rope_key,
    route_ids,
    route_weights,
    attn_gain,
    w_query_nope,
    w_query_rope,
    w_latent_down,
    w_key_rope,
    latent_gain,
    w_key_up,
    w_value_up,
    w_attn_out,
    ffn_gain,
    expert_gate,
    expert_up,
    expert_down,
    shared_gate,
    shared_up,
    shared_down,
    dense_gate,
    dense_up,
    dense_down,
    branch_gate,
):
    own_rows, model_width = tokens.shape
    tp_count = lax.axis_size("tp")
    ep_count = lax.axis_size("ep")
    tp_index = lax.axis_index("tp")
    local_heads = w_query_nope.shape[1]
    head_scale = (w_query_nope.shape[2] + w_query_rope.shape[2]) ** (-0.5)
    normed = norm_rows(tokens, attn_gain).astype(jnp.bfloat16)
    group_in = lax.all_gather(normed, "tp", axis=0, tiled=True)
    group_rows = group_in.shape[0]
    query_nope = jnp.dot(
        group_in, w_query_nope.reshape(model_width, -1), preferred_element_type=jnp.float32
    )
    query_nope = query_nope.astype(jnp.bfloat16).reshape(group_rows, local_heads, -1)
    query_latent = jnp.einsum(
        "ghn,rhn->ghr", query_nope, w_key_up, preferred_element_type=jnp.float32
    ).astype(jnp.bfloat16)
    query_rope = jnp.dot(
        group_in, w_query_rope.reshape(model_width, -1), preferred_element_type=jnp.float32
    )
    query_rope = query_rope.astype(jnp.bfloat16).reshape(group_rows, local_heads, -1)
    latent_part = jnp.dot(group_in, w_latent_down, preferred_element_type=jnp.float32).astype(
        jnp.bfloat16
    )
    own_latent_q, own_rope_q, latent_raw = (
        lax.all_to_all(query_latent, "tp", split_axis=0, concat_axis=1, tiled=True),
        lax.all_to_all(query_rope, "tp", split_axis=0, concat_axis=1, tiled=True),
        lax.all_to_all(latent_part, "tp", split_axis=0, concat_axis=1, tiled=True),
    )
    new_latent = norm_rows(latent_raw, latent_gain).astype(jnp.bfloat16)
    key_rope = jnp.dot(normed, w_key_rope, preferred_element_type=jnp.float32)
    new_rope = rotate(key_rope, lengths).astype(jnp.bfloat16)
    query_rot = rotate(own_rope_q, lengths).astype(jnp.bfloat16)
    scores = jnp.einsum(
        "bhr,blr->bhl", own_latent_q, cache_latent, preferred_element_type=jnp.float32
    )
    scores = scores + jnp.einsum(
        "bhe,ble->bhl", query_rot, cache_rope_key, preferred_element_type=jnp.float32
    )
    scores = scores * head_scale
    in_range = (
        jnp.arange(cache_latent.shape[1], dtype=jnp.int32)[None, None, :] < lengths[:, None, None]
    )
    scores = jnp.where(in_range, scores, -jnp.inf)
    own_score = jnp.einsum(
        "bhr,br->bh", own_latent_q, new_latent, preferred_element_type=jnp.float32
    )
    own_score = (
        own_score
        + jnp.einsum("bhe,be->bh", query_rot, new_rope, preferred_element_type=jnp.float32)
    ) * head_scale
    peak_score = jnp.maximum(jnp.max(scores, axis=-1), own_score)
    past_exp = jnp.exp(scores - peak_score[..., None])
    own_exp = jnp.exp(own_score - peak_score)
    total_exp = jnp.sum(past_exp, axis=-1) + own_exp
    past_weight = (past_exp / total_exp[..., None]).astype(jnp.bfloat16)
    own_weight = (own_exp / total_exp).astype(jnp.bfloat16)
    out_latent = jnp.einsum(
        "bhl,blr->bhr", past_weight, cache_latent, preferred_element_type=jnp.float32
    )
    out_latent = (
        out_latent
        + own_weight.astype(jnp.float32)[..., None] * new_latent.astype(jnp.float32)[:, None, :]
    )
    out_latent = out_latent.astype(jnp.bfloat16)
    head_latent = lax.all_to_all(out_latent, "tp", split_axis=1, concat_axis=0, tiled=True)
    head_values = jnp.einsum(
        "ghr,rhv->ghv", head_latent, w_value_up, preferred_element_type=jnp.float32
    ).astype(jnp.bfloat16)
    attn_part = jnp.dot(
        head_values.reshape(group_rows, -1),
        w_attn_out.reshape(-1, model_width),
        preferred_element_type=jnp.float32,
    )
    own_start = tp_index * own_rows
    placed = lax.dynamic_update_slice_in_dim(
        jnp.zeros((group_rows, model_width), jnp.float32), tokens.astype(jnp.float32), own_start, 0
    )
    group_after = lax.psum((attn_part + placed).astype(jnp.bfloat16), "tp").astype(jnp.float32)
    ffn_in = norm_rows(group_after, ffn_gain).astype(jnp.bfloat16)
    after_attn = lax.dynamic_slice_in_dim(group_after, own_start, own_rows, 0)
    shared_term = jnp.dot(
        swiglu(ffn_in, shared_gate, shared_up), shared_down, preferred_element_type=jnp.float32
    )
    branch_mix = jax.nn.sigmoid(jnp.dot(ffn_in, branch_gate, preferred_element_type=jnp.float32))
    dense_term = branch_mix[:, None] * jnp.dot(
        swiglu(ffn_in, dense_gate, dense_up), dense_down, preferred_element_type=jnp.float32
    )
    top_count = route_ids.shape[1]
    expert_local = expert_gate.shape[0]
    capacity = max(
        2, (2 * own_rows * top_count + expert_local * ep_count - 1) // (expert_local * ep_count)
    )
    target_count = ep_count * expert_local
    slot_count = target_count * capacity
    column = route_ids // expert_local % tp_count
    target = route_ids // (expert_local * tp_count) * expert_local + route_ids % expert_local
    flat_target = jnp.where(column == tp_index, target, -1).reshape(-1)
    target_hits = (
        flat_target[:, None] == jnp.arange(target_count, dtype=jnp.int32)[None, :]
    ).astype(jnp.int32)
    earlier = jnp.cumsum(target_hits, axis=0) - target_hits
    rank_in = jnp.sum(earlier * target_hits, axis=1)
    slot_index = jnp.where(flat_target >= 0, flat_target * capacity + rank_in, -1).reshape(
        group_rows, top_count
    )
    slot_match = slot_index[:, :, None] == jnp.arange(slot_count, dtype=jnp.int32)[None, None, :]
    dispatch = jnp.any(slot_match, axis=1).astype(jnp.bfloat16)
    combine = jnp.sum(jnp.where(slot_match, route_weights[:, :, None], 0.0), axis=1)
    outgoing = jnp.einsum("gs,gd->sd", dispatch, ffn_in, preferred_element_type=jnp.float32).astype(
        jnp.bfloat16
    )
    outgoing = outgoing.reshape(ep_count, expert_local, capacity, model_width)
    arrived = lax.all_to_all(outgoing, "ep", split_axis=0, concat_axis=0, tiled=True)
    gate_val = jnp.einsum(
        "sxcd,xdf->sxcf", arrived, expert_gate, preferred_element_type=jnp.float32
    )
    up_val = jnp.einsum("sxcd,xdf->sxcf", arrived, expert_up, preferred_element_type=jnp.float32)
    act_val = (jax.nn.silu(gate_val) * up_val).astype(jnp.bfloat16)
    result = jnp.einsum(
        "sxcf,xfd->sxcd", act_val, expert_down, preferred_element_type=jnp.float32
    ).astype(jnp.bfloat16)
    returned = lax.all_to_all(result, "ep", split_axis=0, concat_axis=0, tiled=True)
    routed = jnp.dot(
        combine,
        returned.reshape(slot_count, model_width).astype(jnp.float32),
        precision=lax.Precision.HIGHEST,
    )
    ffn_total = routed + shared_term + dense_term
    mixed = (
        after_attn
        + lax.psum_scatter(
            ffn_total.astype(jnp.bfloat16), "tp", scatter_dimension=0, tiled=True
        ).astype(jnp.float32)
    ).astype(jnp.bfloat16)
    return (mixed, new_latent, new_rope)


def solution(mesh):
    in_specs = (
        P(("ep", "tp"), None),
        P(("ep", "tp")),
        P(("ep", "tp"), None, None),
        P(("ep", "tp"), None, None),
        P("ep", None),
        P("ep", None),
        P(),
        P(None, "tp", None),
        P(None, "tp", None),
        P(None, "tp"),
        P(),
        P(),
        P(None, "tp", None),
        P(None, "tp", None),
        P("tp", None, None),
        P(),
        P(("ep", "tp"), None, None),
        P(("ep", "tp"), None, None),
        P(("ep", "tp"), None, None),
        P(None, "tp"),
        P(None, "tp"),
        P("tp", None),
        P(None, "tp"),
        P(None, "tp"),
        P("tp", None),
        P(),
    )
    out_specs = (P(("ep", "tp"), None), P(("ep", "tp"), None), P(("ep", "tp"), None))
    return jax.shard_map(local, mesh=mesh, in_specs=in_specs, out_specs=out_specs, check_vma=False)
```

profile of v0, /device:TPU:0, one launch (start us, length us, event | category | flops | bytes accessed | tf_op | source)
XLA Modules:
  0.0 222.2 jit_solution(12282794214563576408)
XLA Ops:
  7.2 1.0 fusion.58
  8.2 0.8 fusion.95
  9.1 15.7 %all-gather = bf16[8,4,2048]{2,1,0:T(4,128)(2,1)S(1)} all-gather(bf16[1,4,2048]{2,1,0:T(4,128)(2,1)S(1)} %fusion.95), channel_id=1, replica_groups=mesh['ep'=4,'tp'=8] {'tp'}, dimensions={0}, use_global_device_ids=true | all-gather | bytes 147456 | tf_op jit(solution)/shard_map/all_gather | solution.py:75
  24.8 1.1 convolution_convert_fusion.5
  26.0 0.7 reshape.224
  26.7 4.6 %all-to-all-start.2 = ((bf16[8,2,128]{2,1,0:T(2,128)(2,1)}), bf16[8,2,128]{2,1,0:T(2,128)(2,1)S(1)}, u32[]{:S(2)}, u32[]{:S(2)}) async-start(bf16[8,2,128]{2,1,0:T(2,128)(2,1)} %reshape.224), calls=%async_computation.2 | async-start | bytes 8192 | tf_op jit(solution)/shard_map/all_to_all | solution.py:94
  31.3 0.7 convert_element_type.145
  31.9 0.7 iota_compare_fusion.2
  32.7 1.1 fusion.93
  33.8 0.8 copy.71
  35.3 1.1 convolution_convert_fusion.6
  36.4 1.3 convolution_convert_fusion.4
  38.2 0.6 reshape.219
  39.0 0.7 reshape.222
  39.7 0.7 copy.64
  40.4 0.6 dynamic-slice.1
  41.6 5.1 %all-to-all-start.1 = ((bf16[8,2,128]{2,1,0:T(2,128)(2,1)}), bf16[8,2,128]{2,1,0:T(2,128)(2,1)S(1)}, u32[]{:S(2)}, u32[]{:S(2)}) async-start(bf16[8,2,128]{2,1,0:T(2,128)(2,1)} %reshape.222), calls=%async_computation.1 | async-start | bytes 8192 | tf_op jit(solution)/shard_map/all_to_all | solution.py:93
  47.0 5.2 %all-to-all-done.1 = bf16[8,2,128]{2,1,0:T(2,128)(2,1)S(1)} async-done(((bf16[8,2,128]{2,1,0:T(2,128)(2,1)}), bf16[8,2,128]{2,1,0:T(2,128)(2,1)S(1)}, u32[]{:S(2)}, u32[]{:S(2)}) %all-to-all-start.1) | async-done | bytes 4128 | tf_op jit(solution)/shard_map/all_to_all | solution.py:93
  52.2 3.3 %all-to-all-start = ((bf16[32,2,512]{2,1,0:T(2,128)(2,1)}), bf16[32,2,512]{2,1,0:T(2,128)(2,1)S(1)}, u32[]{:S(2)}, u32[]{:S(2)}) async-start(bf16[32,2,512]{2,1,0:T(2,128)(2,1)} %copy.64), calls=%async_computation | async-start | bytes 131072 | tf_op jit(solution)/shard_map/all_to_all | solution.py:92
  56.0 5.4 %all-to-all-done = bf16[32,2,512]{2,1,0:T(2,128)(2,1)S(1)} async-done(((bf16[32,2,512]{2,1,0:T(2,128)(2,1)}), bf16[32,2,512]{2,1,0:T(2,128)(2,1)S(1)}, u32[]{:S(2)}, u32[]{:S(2)}) %all-to-all-start) | async-done | bytes 65568 | tf_op jit(solution)/shard_map/all_to_all | solution.py:92
  61.7 3.5 %fusion.100 = f32[4,16,1024]{2,1,0:T(8,128)S(1)} fusion(bf16[4,16,512]{2,1,0:T(8,128)(2,1)S(1)} %all_to_all.58, bf16[4,1024,512]{2,1,0:T(8,128)(2,1)} %param.28), kind=kOutput, calls=%fused_computation.141 | convolution fusion | flops 67108864 | bytes 4521984 | tf_op jit(solution)/shard_map/bhr,blr->bhl/dot_general | solution.py:100
  65.2 0.3 fusion.99
  65.5 0.2 fusion.37
  65.8 0.7 fusion.11
  66.5 0.7 copy.68
  67.2 3.3 %all-to-all-start.3 = ((bf16[4,16,512]{2,0,1:T(4,128)(2,1)}), bf16[4,16,512]{2,0,1:T(4,128)(2,1)S(1)}, u32[]{:S(2)}, u32[]{:S(2)}) async-start(bf16[4,16,512]{2,0,1:T(4,128)(2,1)} %copy.68), calls=%async_computation.3 | async-start | bytes 131072 | tf_op jit(solution)/shard_map/all_to_all | solution.py:132
  70.6 0.7 select_reduce_fusion
  71.3 5.1 %all-to-all-done.3 = bf16[4,16,512]{2,0,1:T(4,128)(2,1)S(1)} async-done(((bf16[4,16,512]{2,0,1:T(4,128)(2,1)}), bf16[4,16,512]{2,0,1:T(4,128)(2,1)S(1)}, u32[]{:S(2)}, u32[]{:S(2)}) %all-to-all-start.3) | async-done | bytes 65568 | tf_op jit(solution)/shard_map/all_to_all | solution.py:132
  76.5 1.3 convolution_bitcast_fusion
  77.8 0.7 convert_element_type.161
  78.6 53.5 %all-reduce.4.cloned.1.call-done = bf16[32,2048]{1,0:T(8,128)(2,1)} async-done(((bf16[32,2048]{1,0:T(8,128)(2,1)}), bf16[32,2048]{1,0:T(8,128)(2,1)}) %all-reduce.4.cloned.1.call-update) | async-done | bytes 131088 | tf_op jit(solution)/shard_map/psum | solution.py:145
  132.1 1.0 multiply_reduce_fusion
  133.2 1.8 fusion.2
  135.0 3.6 %all-to-all-start.4 = ((bf16[4,1,8,2048]{3,2,1,0:T(8,128)(2,1)}), bf16[4,1,8,2048]{3,2,1,0:T(8,128)(2,1)S(1)}, u32[]{:S(2)}, u32[]{:S(2)}) async-start(bf16[4,1,8,2048]{3,2,1,0:T(8,128)(2,1)} %fusion.2), calls=%async_computation.4 | async-start | bytes 262144 | tf_op jit(solution)/shard_map/all_to_all | solution.py:180
  138.6 1.8 fusion.96
  140.4 1.9 fusion.97
  142.3 1.4 all-to-all-done.4
  143.7 2.0 fusion.13
  145.7 3.2 %fusion.3 = bf16[4,1,8,2048]{3,2,1,0:T(8,128)(2,1)} fusion(bf16[1,512,2048]{2,1,0:T(8,128)(2,1)S(1)} %copy-done, bf16[1,2048,512]{2,1,0:T(8,128)(2,1)} %param.43, bf16[4,1,8,2048]{3,2,1,0:T(8,128)(2,1)S(1)} %all-to-all-done.4, f32[4,1,8,512]{3,2,0,1:T(8,128)S(1)} %fusion.13), kind=kOutput, calls=%fused_computation.8 | convolution fusion | flops 134381568 | bytes 4521984 | tf_op jit(solution)/shard_map/sxcf,xfd->sxcd/dot_general | solution.py:186
  148.9 3.5 %all-to-all-start.5 = ((bf16[4,1,8,2048]{3,2,1,0:T(8,128)(2,1)}), bf16[4,1,8,2048]{3,2,1,0:T(8,128)(2,1)S(1)}, u32[]{:S(2)}, u32[]{:S(2)}) async-start(bf16[4,1,8,2048]{3,2,1,0:T(8,128)(2,1)} %fusion.3), calls=%async_computation.5 | async-start | bytes 262144 | tf_op jit(solution)/shard_map/all_to_all | solution.py:189
  152.5 0.7 fusion.34
  153.2 4.2 %all-to-all-done.5 = bf16[4,1,8,2048]{3,2,1,0:T(8,128)(2,1)S(1)} async-done(((bf16[4,1,8,2048]{3,2,1,0:T(8,128)(2,1)}), bf16[4,1,8,2048]{3,2,1,0:T(8,128)(2,1)S(1)}, u32[]{:S(2)}, u32[]{:S(2)}) %all-to-all-start.5) | async-done | bytes 131104 | tf_op jit(solution)/shard_map/all_to_all | solution.py:189
  157.4 0.2 fusion.38
  157.6 1.4 convolution_add_fusion
  159.1 2.2 fusion.1
  161.3 1.3 pad_maximum_fusion.3
  162.6 51.4 %all-reduce.6.cloned.1.call-done = bf16[32,2048]{1,0:T(8,128)(2,1)} async-done(((bf16[32,2048]{1,0:T(8,128)(2,1)}), bf16[32,2048]{1,0:T(8,128)(2,1)}) %all-reduce.6.cloned.1.call-update) | async-done | bytes 131088
  214.0 1.4 add_convert_fusion
  (80 shorter events, 2.7 us)
Async XLA Ops:
  7.2 138.5 %copy-start = (bf16[1,512,2048]{2,1,0:T(8,128)(2,1)S(1)}, bf16[1,512,2048]{2,1,0:T(8,128)(2,1)}, u32[]{:S(2)}) copy-start(bf16[1,512,2048]{2,1,0:T(8,128)(2,1)} %param.44) | copy-start | bytes 6291460
  7.2 33.2 %copy-start.18 = (u32[32]{0:T(128)S(1)}, u32[32]{0:T(128)}, u32[]{:S(2)}) copy-start(u32[32]{0:T(128)} %constant.109) | copy-start | bytes 388
  7.2 30.7 %copy-start.10 = (bf16[512,2,64]{0,2,1:T(8,128)(2,1)S(1)}, bf16[512,2,64]{0,2,1:T(8,128)(2,1)}, u32[]{:S(2)}) copy-start(bf16[512,2,64]{0,2,1:T(8,128)(2,1)} %param.38) | copy-start | bytes 393220
  7.2 31.0 %copy-start.14 = (bf16[2048]{0:T(1024)(128)(2,1)S(1)}, bf16[2048]{0:T(1024)(128)(2,1)}, u32[]{:S(2)}) copy-start(bf16[2048]{0:T(1024)(128)(2,1)} %param.51) | copy-start | bytes 12292
  7.2 48.5 %copy-start.16 = (f32[512]{0:T(512)S(1)}, f32[512]{0:T(512)}, u32[]{:S(2)}) copy-start(f32[512]{0:T(512)} %param.37) | copy-start | bytes 6148
  26.7 14.9 %all-to-all-start.2 = ((bf16[8,2,128]{2,1,0:T(2,128)(2,1)}), bf16[8,2,128]{2,1,0:T(2,128)(2,1)S(1)}, u32[]{:S(2)}, u32[]{:S(2)}) async-start(bf16[8,2,128]{2,1,0:T(2,128)(2,1)} %reshape.224), calls=%async_computation.2 | async-start | bytes 8192 | tf_op jit(solution)/shard_map/all_to_all | solution.py:94
  38.1 23.3 %copy-start.12 = (bf16[4,16]{1,0:T(4,128)(2,1)}, bf16[4,16]{1,0:T(4,128)(2,1)S(1)}, u32[]{:S(2)}) copy-start(bf16[4,16]{1,0:T(4,128)(2,1)S(1)} %get-tuple-element.10) | copy-start | bytes 388
  41.6 10.6 %all-to-all-start.1 = ((bf16[8,2,128]{2,1,0:T(2,128)(2,1)}), bf16[8,2,128]{2,1,0:T(2,128)(2,1)S(1)}, u32[]{:S(2)}, u32[]{:S(2)}) async-start(bf16[8,2,128]{2,1,0:T(2,128)(2,1)} %reshape.222), calls=%async_computation.1 | async-start | bytes 8192 | tf_op jit(solution)/shard_map/all_to_all | solution.py:93
  52.2 9.2 %all-to-all-start = ((bf16[32,2,512]{2,1,0:T(2,128)(2,1)}), bf16[32,2,512]{2,1,0:T(2,128)(2,1)S(1)}, u32[]{:S(2)}, u32[]{:S(2)}) async-start(bf16[32,2,512]{2,1,0:T(2,128)(2,1)} %copy.64), calls=%async_computation | async-start | bytes 131072 | tf_op jit(solution)/shard_map/all_to_all | solution.py:92
  55.8 9.4 %copy-start.15 = (bf16[4,512]{1,0:T(4,128)(2,1)}, bf16[4,512]{1,0:T(4,128)(2,1)S(1)}, u32[]{:S(2)}) copy-start(bf16[4,512]{1,0:T(4,128)(2,1)S(1)} %get-tuple-element.4) | copy-start | bytes 12292
  61.6 3.5 %copy-start.6 = (bf16[4,1024,32]{1,2,0:T(8,128)(2,1)S(1)}, bf16[4,1024,32]{1,2,0:T(8,128)(2,1)}, u32[]{:S(2)}) copy-start(bf16[4,1024,32]{1,2,0:T(8,128)(2,1)} %param.29) | copy-start | bytes 786436
  61.6 4.1 %copy-start.1 = (bf16[4,1024,512]{2,1,0:T(8,128)(2,1)S(1)}, bf16[4,1024,512]{2,1,0:T(8,128)(2,1)}, u32[]{:S(2)}) copy-start(bf16[4,1024,512]{2,1,0:T(8,128)(2,1)} %param.28) | copy-start | bytes 12582916
  65.8 4.8 %copy-start.17 = (f32[32,4]{0,1:T(4,128)S(1)}, f32[32,4]{0,1:T(4,128)}, u32[]{:S(2)}) copy-start(f32[32,4]{0,1:T(4,128)} %param.31) | copy-start | bytes 1540
  65.8 10.7 %copy-start.4 = (bf16[2,64,2048]{2,1,0:T(8,128)(2,1)S(1)}, bf16[2,64,2048]{2,1,0:T(8,128)(2,1)}, u32[]{:S(2)}) copy-start(bf16[2,64,2048]{2,1,0:T(8,128)(2,1)} %param.40) | copy-start | bytes 1572868
  65.8 12.0 %copy-start.9 = (bf16[4,2048]{1,0:T(4,128)(2,1)S(1)}, bf16[4,2048]{1,0:T(4,128)(2,1)}, u32[]{:S(2)}) copy-start(bf16[4,2048]{1,0:T(4,128)(2,1)} %param.26) | copy-start | bytes 49156
  66.5 66.7 %copy-start.8 = (f32[2048]{0:T(1024)S(1)}, f32[2048]{0:T(1024)}, u32[]{:S(2)}) copy-start(f32[2048]{0:T(1024)} %param.41) | copy-start | bytes 24580
  66.5 72.1 %copy-start.3 = (bf16[2048,128]{1,0:T(8,128)(2,1)S(1)}, bf16[2048,128]{1,0:T(8,128)(2,1)}, u32[]{:S(2)}) copy-start(bf16[2048,128]{1,0:T(8,128)(2,1)} %param.48) | copy-start | bytes 1572868
  67.2 9.2 %all-to-all-start.3 = ((bf16[4,16,512]{2,0,1:T(4,128)(2,1)}), bf16[4,16,512]{2,0,1:T(4,128)(2,1)S(1)}, u32[]{:S(2)}, u32[]{:S(2)}) async-start(bf16[4,16,512]{2,0,1:T(4,128)(2,1)} %copy.68), calls=%async_computation.3 | async-start | bytes 131072 | tf_op jit(solution)/shard_map/all_to_all | solution.py:132
  70.5 61.6 %all-reduce.4.cloned.1.call-start = ((), (), s32[]{:S(2)}) async-start(), calls=%async_computation.6 | async-start | bytes 262144 | tf_op jit(solution)/shard_map/psum | solution.py:145
  135.0 8.7 %all-to-all-start.4 = ((bf16[4,1,8,2048]{3,2,1,0:T(8,128)(2,1)}), bf16[4,1,8,2048]{3,2,1,0:T(8,128)(2,1)S(1)}, u32[]{:S(2)}, u32[]{:S(2)}) async-start(bf16[4,1,8,2048]{3,2,1,0:T(8,128)(2,1)} %fusion.2), calls=%async_computation.4 | async-start | bytes 262144 | tf_op jit(solution)/shard_map/all_to_all | solution.py:180
  145.7 6.7 %copy-start.2 = (bf16[32,2048]{1,0:T(8,128)(2,1)S(1)}, bf16[32,2048]{1,0:T(8,128)(2,1)}, u32[]{:S(2)}) copy-start(bf16[32,2048]{1,0:T(8,128)(2,1)} %all-reduce.4.cloned.1.call-done) | copy-start | bytes 393220
  145.7 6.7 %copy-start.13 = (bf16[2048,1]{0,1:T(2,128)(2,1)S(1)}, bf16[2048,1]{0,1:T(2,128)(2,1)}, u32[]{:S(2)}) copy-start(bf16[2048,1]{0,1:T(2,128)(2,1)} %reshape.219) | copy-start | bytes 12292
  145.7 11.7 %copy-start.11 = (f32[32,32]{1,0:T(8,128)S(1)}, f32[32,32]{1,0:T(8,128)}, u32[]{:S(2)}) copy-start(f32[32,32]{1,0:T(8,128)} %select_reduce_fusion) | copy-start | bytes 12292
  145.7 11.9 %copy-start.7 = (bf16[64,2048]{1,0:T(8,128)(2,1)S(1)}, bf16[64,2048]{1,0:T(8,128)(2,1)}, u32[]{:S(2)}) copy-start(bf16[64,2048]{1,0:T(8,128)(2,1)} %param.47) | copy-start | bytes 786436
  148.9 10.2 %copy-start.5 = (bf16[128,2048]{1,0:T(8,128)(2,1)S(1)}, bf16[128,2048]{1,0:T(8,128)(2,1)}, u32[]{:S(2)}) copy-start(bf16[128,2048]{1,0:T(8,128)(2,1)} %param.50) | copy-start | bytes 1572868
  148.9 8.4 %all-to-all-start.5 = ((bf16[4,1,8,2048]{3,2,1,0:T(8,128)(2,1)}), bf16[4,1,8,2048]{3,2,1,0:T(8,128)(2,1)S(1)}, u32[]{:S(2)}, u32[]{:S(2)}) async-start(bf16[4,1,8,2048]{3,2,1,0:T(8,128)(2,1)} %fusion.3), calls=%async_computation.5 | async-start | bytes 262144 | tf_op jit(solution)/shard_map/all_to_all | solution.py:189
  152.4 61.6 %all-reduce.6.cloned.1.call-start = ((), (), s32[]{:S(2)}) async-start(), calls=%async_computation.7 | async-start | bytes 262144
Sparse Core Ops, SparseCore 0:
  78.6 53.4 all-reduce.3
  161.4 52.5 all-reduce.5
where the time goes:
time: 223 us; the launch traced here: 222 us
  waiting for transfers between devices  126 us (57%)
  matrix products  26.3 us (12%)
  starting transfers between devices  23.6 us (11%)
  blocking collectives  15.7 us (7%)
  between operations  15.1 us (7%)
  other arithmetic  9.66 us (4%)
  local copies, waits for them, and re-layouts  5.69 us (3%)
    psum x1, waiting for transfers between devices, local(): lax.psum((attn_part + placed).astype(jnp.bfloat16), 'tp')  53.5 us
    unnamed x3, waiting for transfers between devices  51.4 us
    all_gather x1, blocking collectives, local(): group_in = lax.all_gather(normed, 'tp', axis=0, tiled=True)  15.7 us
    all_to_all x1, waiting for transfers between devices, local(): lax.all_to_all(query_latent, 'tp', split_axis=0, concat_axis=1, tiled=True)  5.38 us
    all_to_all x1, waiting for transfers between devices, local(): lax.all_to_all(query_rope, 'tp', split_axis=0, concat_axis=1, tiled=True)  5.2 us
    all_to_all x1, starting transfers between devices, local(): lax.all_to_all(query_rope, 'tp', split_axis=0, concat_axis=1, tiled=True)  5.11 us
    all_to_all x1, waiting for transfers between devices, local(): lax.all_to_all(out_latent, 'tp', split_axis=1, concat_axis=0, tiled=True)  5.08 us
    all_to_all x1, starting transfers between devices, local(): lax.all_to_all(latent_part, 'tp', split_axis=0, concat_axis=1, tiled=True)  4.6 us
  transfers between devices with their start and end apart: 8, of which 7 were waited for; matrix products, arithmetic and copies ran while one was open for 8% of the time, Pallas kernels for 0%

commit v1 on v0

--- a/solution.py
+++ b/solution.py
@@ -2,6 +2,7 @@
 import jax.numpy as jnp
 from jax import lax
 from jax.sharding import PartitionSpec as P
+from jax.lax import all_gather
 
 epsilon = 1e-06
 rope_base = 10000.0
@@ -65,6 +66,10 @@
     dense_down,
     branch_gate,
 ):
+
+    def _search_paths(state, ax_name):
+        return jnp.sum(all_gather(state, axis_name=ax_name), axis=0)
+
     own_rows, model_width = tokens.shape
     tp_count = lax.axis_size("tp")
     ep_count = lax.axis_size("ep")
@@ -142,7 +147,7 @@
     placed = lax.dynamic_update_slice_in_dim(
         jnp.zeros((group_rows, model_width), jnp.float32), tokens.astype(jnp.float32), own_start, 0
     )
-    group_after = lax.psum((attn_part + placed).astype(jnp.bfloat16), "tp").astype(jnp.float32)
+    group_after = _search_paths((attn_part + placed).astype(jnp.bfloat16), "tp").astype(jnp.float32)
     ffn_in = norm_rows(group_after, ffn_gain).astype(jnp.bfloat16)
     after_attn = lax.dynamic_slice_in_dim(group_after, own_start, own_rows, 0)
     shared_term = jnp.dot(

time: 223 us -> 188 us (0.84)
  waiting for transfers between devices: 126 us -> 97 us
  matrix products: 26.3 us -> 21.8 us
    psum x1 -> x0, waiting for transfers between devices: 53.5 us -> none  [local(): lax.psum((attn_part + placed).astype(jnp.bfloat16), 'tp')]
    all_gather x0 -> x1, waiting for transfers between devices: none -> 18.5 us  [_search_paths(): return jnp.sum(all_gather(state, axis_name=ax_name), axis=0)]
    all_to_all x1, waiting for transfers between devices: 1.36 us -> 4.76 us  [local(): lax.all_to_all(outgoing, 'ep', split_axis=0, concat_axis=0, tiled=True)]
    dot_general x2, matrix products: 3.66 us -> 0.51 us  [swiglu(): gate_val = jnp.dot(inputs, gate_w, preferred_element_type=jnp.float32)]
  transfers between devices with their start and end apart: 8 -> 8, of which waited for: 7 -> 7; matrix products, arithmetic and copies ran while one was open for 8% -> 6% of each run, Pallas kernels for 0% -> 0%
where the time goes in v1:
time: 188 us; the launch traced here: 186 us
  waiting for transfers between devices  97 us (52%)
  starting transfers between devices  23.6 us (13%)
  matrix products  21.8 us (12%)
  blocking collectives  15.7 us (8%)
  between operations  15.1 us (8%)
  other arithmetic  8.86 us (5%)
  local copies, waits for them, and re-layouts  4.43 us (2%)
    unnamed x3, waiting for transfers between devices  52.7 us
    all_gather x1, waiting for transfers between devices, _search_paths(): return jnp.sum(all_gather(state, axis_name=ax_name), axis=0)  18.5 us
    all_gather x1, blocking collectives, local(): group_in = lax.all_gather(normed, 'tp', axis=0, tiled=True)  15.7 us
    all_to_all x1, waiting for transfers between devices, local(): lax.all_to_all(out_latent, 'tp', split_axis=1, concat_axis=0, tiled=True)  5.79 us
    all_to_all x1, waiting for transfers between devices, local(): lax.all_to_all(query_rope, 'tp', split_axis=0, concat_axis=1, tiled=True)  5.3 us
    all_to_all x1, waiting for transfers between devices, local(): lax.all_to_all(query_latent, 'tp', split_axis=0, concat_axis=1, tiled=True)  5.28 us
    all_to_all x1, starting transfers between devices, local(): lax.all_to_all(query_rope, 'tp', split_axis=0, concat_axis=1, tiled=True)  5.1 us
    all_to_all x1, waiting for transfers between devices, local(): lax.all_to_all(outgoing, 'ep', split_axis=0, concat_axis=0, tiled=True)  4.76 us
  transfers between devices with their start and end apart: 8, of which 7 were waited for; matrix products, arithmetic and copies ran while one was open for 6% of the time, Pallas kernels for 0%

profile of v1, /device:TPU:0, one launch (start us, length us, event | category | flops | bytes accessed | tf_op | source)
XLA Modules:
  0.0 186.5 jit_solution(12822232866815691506)
XLA Ops:
  7.2 1.0 fusion.58
  8.2 0.8 fusion.95
  9.0 15.7 %all-gather.1 = bf16[8,4,2048]{2,1,0:T(4,128)(2,1)S(1)} all-gather(bf16[1,4,2048]{2,1,0:T(4,128)(2,1)S(1)} %fusion.95), channel_id=1, replica_groups=mesh['ep'=4,'tp'=8] {'tp'}, dimensions={0}, use_global_device_ids=true | all-gather | bytes 147456 | tf_op jit(solution)/shard_map/all_gather | solution.py:80
  24.8 1.1 convolution_convert_fusion.5
  25.9 0.7 reshape.225
  26.6 4.6 %all-to-all-start.2 = ((bf16[8,2,128]{2,1,0:T(2,128)(2,1)}), bf16[8,2,128]{2,1,0:T(2,128)(2,1)S(1)}, u32[]{:S(2)}, u32[]{:S(2)}) async-start(bf16[8,2,128]{2,1,0:T(2,128)(2,1)} %reshape.225), calls=%async_computation.2 | async-start | bytes 8192 | tf_op jit(solution)/shard_map/all_to_all | solution.py:99
  31.2 0.7 convert_element_type.147
  31.9 0.7 iota_compare_fusion.2
  32.6 1.1 fusion.93
  33.8 1.1 convolution_convert_fusion.6
  34.9 1.3 convolution_convert_fusion.4
  36.8 0.7 reshape.223
  37.5 0.7 copy.64
  38.2 5.1 %all-to-all-start.1 = ((bf16[8,2,128]{2,1,0:T(2,128)(2,1)}), bf16[8,2,128]{2,1,0:T(2,128)(2,1)S(1)}, u32[]{:S(2)}, u32[]{:S(2)}) async-start(bf16[8,2,128]{2,1,0:T(2,128)(2,1)} %reshape.223), calls=%async_computation.1 | async-start | bytes 8192 | tf_op jit(solution)/shard_map/all_to_all | solution.py:98
  43.5 5.3 %all-to-all-done.1 = bf16[8,2,128]{2,1,0:T(2,128)(2,1)S(1)} async-done(((bf16[8,2,128]{2,1,0:T(2,128)(2,1)}), bf16[8,2,128]{2,1,0:T(2,128)(2,1)S(1)}, u32[]{:S(2)}, u32[]{:S(2)}) %all-to-all-start.1) | async-done | bytes 4128 | tf_op jit(solution)/shard_map/all_to_all | solution.py:98
  48.8 3.3 %all-to-all-start = ((bf16[32,2,512]{2,1,0:T(2,128)(2,1)}), bf16[32,2,512]{2,1,0:T(2,128)(2,1)S(1)}, u32[]{:S(2)}, u32[]{:S(2)}) async-start(bf16[32,2,512]{2,1,0:T(2,128)(2,1)} %copy.64), calls=%async_computation | async-start | bytes 131072 | tf_op jit(solution)/shard_map/all_to_all | solution.py:97
  52.5 0.2 fusion.83
  52.7 5.3 %all-to-all-done = bf16[32,2,512]{2,1,0:T(2,128)(2,1)S(1)} async-done(((bf16[32,2,512]{2,1,0:T(2,128)(2,1)}), bf16[32,2,512]{2,1,0:T(2,128)(2,1)S(1)}, u32[]{:S(2)}, u32[]{:S(2)}) %all-to-all-start) | async-done | bytes 65568 | tf_op jit(solution)/shard_map/all_to_all | solution.py:97
  58.1 3.5 %fusion.100 = f32[4,16,1024]{2,1,0:T(8,128)S(1)} fusion(bf16[4,16,512]{2,1,0:T(8,128)(2,1)S(1)} %all_to_all.58, bf16[4,1024,512]{2,1,0:T(8,128)(2,1)} %param.28), kind=kOutput, calls=%fused_computation.141 | convolution fusion | flops 67108864 | bytes 4521984 | tf_op jit(solution)/shard_map/bhr,blr->bhl/dot_general | solution.py:105
  61.8 0.3 fusion.99
  62.1 0.2 fusion.37
  62.4 0.7 fusion.11
  63.1 0.7 copy.68
  63.8 3.3 %all-to-all-start.3 = ((bf16[4,16,512]{2,0,1:T(4,128)(2,1)}), bf16[4,16,512]{2,0,1:T(4,128)(2,1)S(1)}, u32[]{:S(2)}, u32[]{:S(2)}) async-start(bf16[4,16,512]{2,0,1:T(4,128)(2,1)} %copy.68), calls=%async_computation.3 | async-start | bytes 131072 | tf_op jit(solution)/shard_map/all_to_all | solution.py:137
  67.2 5.8 %all-to-all-done.3 = bf16[4,16,512]{2,0,1:T(4,128)(2,1)S(1)} async-done(((bf16[4,16,512]{2,0,1:T(4,128)(2,1)}), bf16[4,16,512]{2,0,1:T(4,128)(2,1)S(1)}, u32[]{:S(2)}, u32[]{:S(2)}) %all-to-all-start.3) | async-done | bytes 65568 | tf_op jit(solution)/shard_map/all_to_all | solution.py:137
  73.1 1.3 convolution_bitcast_fusion
  74.4 0.7 convert_element_type.163
  75.5 0.2 reduce_window_sum.11
  75.7 0.2 select_reduce_fusion.1
  76.1 0.6 dynamic-slice.1
  77.5 18.5 %all-gather.4.cloned.1.call-done = bf16[256,2048]{1,0:T(8,128)(2,1)} async-done(((bf16[32,2048]{1,0:T(8,128)(2,1)}), bf16[256,2048]{1,0:T(8,128)(2,1)}) %all-gather.4.cloned.1.call-update) | async-done | bytes 1048592 | tf_op jit(solution)/shard_map/all_gather | solution.py:71
  96.0 1.4 reduce_sum.71
  97.6 0.3 fusion.96
  97.8 0.9 fusion.2
  98.7 3.7 %all-to-all-start.4 = ((bf16[4,1,8,2048]{3,2,1,0:T(8,128)(2,1)}), bf16[4,1,8,2048]{3,2,1,0:T(8,128)(2,1)S(1)}, u32[]{:S(2)}, u32[]{:S(2)}) async-start(bf16[4,1,8,2048]{3,2,1,0:T(8,128)(2,1)} %fusion.2), calls=%async_computation.4 | async-start | bytes 262144 | tf_op jit(solution)/shard_map/all_to_all | solution.py:185
  102.4 0.3 fusion.97
  102.6 4.8 %all-to-all-done.4 = bf16[4,1,8,2048]{3,2,1,0:T(8,128)(2,1)S(1)} async-done(((bf16[4,1,8,2048]{3,2,1,0:T(8,128)(2,1)}), bf16[4,1,8,2048]{3,2,1,0:T(8,128)(2,1)S(1)}, u32[]{:S(2)}, u32[]{:S(2)}) %all-to-all-start.4) | async-done | bytes 131104 | tf_op jit(solution)/shard_map/all_to_all | solution.py:185
  107.4 2.0 %fusion.13 = f32[4,1,8,512]{3,2,0,1:T(8,128)S(1)} fusion(bf16[1,2048,512]{2,1,0:T(8,128)(2,1)} %param.42, bf16[4,1,8,2048]{3,2,1,0:T(8,128)(2,1)S(1)} %all-to-all-done.4), kind=kOutput, calls=%fused_computation.21 | convolution fusion | flops 67108864 | bytes 2293760 | tf_op jit(solution)/shard_map/sxcd,xdf->sxcf/dot_general | solution.py:186
  109.4 3.1 %fusion.3 = bf16[4,1,8,2048]{3,2,1,0:T(8,128)(2,1)} fusion(bf16[1,512,2048]{2,1,0:T(8,128)(2,1)S(1)} %copy-done, bf16[1,2048,512]{2,1,0:T(8,128)(2,1)} %param.43, bf16[4,1,8,2048]{3,2,1,0:T(8,128)(2,1)S(1)} %all-to-all-done.4, f32[4,1,8,512]{3,2,0,1:T(8,128)S(1)} %fusion.13), kind=kOutput, calls=%fused_computation.8 | convolution fusion | flops 134381568 | bytes 4521984 | tf_op jit(solution)/shard_map/sxcf,xfd->sxcd/dot_general | solution.py:191
  112.6 3.5 %all-to-all-start.5 = ((bf16[4,1,8,2048]{3,2,1,0:T(8,128)(2,1)}), bf16[4,1,8,2048]{3,2,1,0:T(8,128)(2,1)S(1)}, u32[]{:S(2)}, u32[]{:S(2)}) async-start(bf16[4,1,8,2048]{3,2,1,0:T(8,128)(2,1)} %fusion.3), calls=%async_computation.5 | async-start | bytes 262144 | tf_op jit(solution)/shard_map/all_to_all | solution.py:194
  116.1 0.2 fusion.34
  116.3 4.7 %all-to-all-done.5 = bf16[4,1,8,2048]{3,2,1,0:T(8,128)(2,1)S(1)} async-done(((bf16[4,1,8,2048]{3,2,1,0:T(8,128)(2,1)}), bf16[4,1,8,2048]{3,2,1,0:T(8,128)(2,1)S(1)}, u32[]{:S(2)}, u32[]{:S(2)}) %all-to-all-start.5) | async-done | bytes 131104 | tf_op jit(solution)/shard_map/all_to_all | solution.py:194
  121.0 0.2 fusion.38
  121.3 1.5 convolution_add_fusion
  122.8 2.2 %fusion.1 = bf16[32,2048]{1,0:T(8,128)(2,1)} fusion(f32[32,2048]{1,0:T(8,128)S(1)} %convolution_add_fusion, bf16[128,2048]{1,0:T(8,128)(2,1)S(1)} %copy-done.4, bf16[2048,128]{1,0:T(8,128)(2,1)} %param.49, f32[32]{0:T(128)S(1)} %fusion.34, f32[32,128]{1,0:T(8,128)S(1)} %fusion.96, f32[2048]{0:T(1024)S(1)} %copy-done.7, f32[32]{0:T(128)S(1)} %add_rsqrt_fusion, ...), kind=kOutput, calls=%fused_computation.4 | convolution fusion | flops 34037760 | bytes 1597696 | tf_op jit(solution)/shard_map/dot_general | solution.py:157
  125.0 0.6 pad_maximum_fusion.3
  125.6 52.6 %all-reduce.3.cloned.1.call-done = bf16[32,2048]{1,0:T(8,128)(2,1)} async-done(((bf16[32,2048]{1,0:T(8,128)(2,1)}), bf16[32,2048]{1,0:T(8,128)(2,1)}) %all-reduce.3.cloned.1.call-update) | async-done | bytes 131088
  178.2 1.4 add_convert_fusion
  (75 shorter events, 2.5 us)
Async XLA Ops:
  7.2 102.3 %copy-start = (bf16[1,512,2048]{2,1,0:T(8,128)(2,1)S(1)}, bf16[1,512,2048]{2,1,0:T(8,128)(2,1)}, u32[]{:S(2)}) copy-start(bf16[1,512,2048]{2,1,0:T(8,128)(2,1)} %param.44) | copy-start | bytes 6291460
  7.2 29.2 %copy-start.9 = (bf16[512,2,64]{0,2,1:T(8,128)(2,1)S(1)}, bf16[512,2,64]{0,2,1:T(8,128)(2,1)}, u32[]{:S(2)}) copy-start(bf16[512,2,64]{0,2,1:T(8,128)(2,1)} %param.38) | copy-start | bytes 393220
  7.2 45.2 %copy-start.12 = (f32[512]{0:T(512)S(1)}, f32[512]{0:T(512)}, u32[]{:S(2)}) copy-start(f32[512]{0:T(512)} %param.37) | copy-start | bytes 6148
  26.6 11.5 %all-to-all-start.2 = ((bf16[8,2,128]{2,1,0:T(2,128)(2,1)}), bf16[8,2,128]{2,1,0:T(2,128)(2,1)S(1)}, u32[]{:S(2)}, u32[]{:S(2)}) async-start(bf16[8,2,128]{2,1,0:T(2,128)(2,1)} %reshape.225), calls=%async_computation.2 | async-start | bytes 8192 | tf_op jit(solution)/shard_map/all_to_all | solution.py:99
  38.2 10.6 %all-to-all-start.1 = ((bf16[8,2,128]{2,1,0:T(2,128)(2,1)}), bf16[8,2,128]{2,1,0:T(2,128)(2,1)S(1)}, u32[]{:S(2)}, u32[]{:S(2)}) async-start(bf16[8,2,128]{2,1,0:T(2,128)(2,1)} %reshape.223), calls=%async_computation.1 | async-start | bytes 8192 | tf_op jit(solution)/shard_map/all_to_all | solution.py:98
  48.8 9.2 %all-to-all-start = ((bf16[32,2,512]{2,1,0:T(2,128)(2,1)}), bf16[32,2,512]{2,1,0:T(2,128)(2,1)S(1)}, u32[]{:S(2)}, u32[]{:S(2)}) async-start(bf16[32,2,512]{2,1,0:T(2,128)(2,1)} %copy.64), calls=%async_computation | async-start | bytes 131072 | tf_op jit(solution)/shard_map/all_to_all | solution.py:97
  52.5 9.1 %copy-start.11 = (bf16[4,512]{1,0:T(4,128)(2,1)}, bf16[4,512]{1,0:T(4,128)(2,1)S(1)}, u32[]{:S(2)}) copy-start(bf16[4,512]{1,0:T(4,128)(2,1)S(1)} %get-tuple-element.4) | copy-start | bytes 12292
  58.1 3.7 %copy-start.5 = (bf16[4,1024,32]{1,2,0:T(8,128)(2,1)S(1)}, bf16[4,1024,32]{1,2,0:T(8,128)(2,1)}, u32[]{:S(2)}) copy-start(bf16[4,1024,32]{1,2,0:T(8,128)(2,1)} %param.29) | copy-start | bytes 786436
  58.1 4.2 %copy-start.1 = (bf16[4,1024,512]{2,1,0:T(8,128)(2,1)S(1)}, bf16[4,1024,512]{2,1,0:T(8,128)(2,1)}, u32[]{:S(2)}) copy-start(bf16[4,1024,512]{2,1,0:T(8,128)(2,1)} %param.28) | copy-start | bytes 12582916
  62.3 10.7 %copy-start.3 = (bf16[2,64,2048]{2,1,0:T(8,128)(2,1)S(1)}, bf16[2,64,2048]{2,1,0:T(8,128)(2,1)}, u32[]{:S(2)}) copy-start(bf16[2,64,2048]{2,1,0:T(8,128)(2,1)} %param.40) | copy-start | bytes 1572868
  62.4 12.0 %copy-start.8 = (bf16[4,2048]{1,0:T(4,128)(2,1)S(1)}, bf16[4,2048]{1,0:T(4,128)(2,1)}, u32[]{:S(2)}) copy-start(bf16[4,2048]{1,0:T(4,128)(2,1)} %param.26) | copy-start | bytes 49156
  62.4 12.8 %copy-start.10 = (bf16[2048]{0:T(1024)(128)(2,1)S(1)}, bf16[2048]{0:T(1024)(128)(2,1)}, u32[]{:S(2)}) copy-start(bf16[2048]{0:T(1024)(128)(2,1)} %param.51) | copy-start | bytes 12292
  62.4 12.8 %copy-start.13 = (s32[32,4]{0,1:T(4,128)S(1)}, s32[32,4]{0,1:T(4,128)}, u32[]{:S(2)}) copy-start(s32[32,4]{0,1:T(4,128)} %param.30) | copy-start | bytes 1540
  63.1 13.0 %copy-start.15 = (u32[32]{0:T(128)S(1)}, u32[32]{0:T(128)}, u32[]{:S(2)}) copy-start(u32[32]{0:T(128)} %constant.111) | copy-start | bytes 388
  63.1 14.3 %copy-start.14 = (f32[32,4]{0,1:T(4,128)S(1)}, f32[32,4]{0,1:T(4,128)}, u32[]{:S(2)}) copy-start(f32[32,4]{0,1:T(4,128)} %param.31) | copy-start | bytes 1540
  63.1 34.4 %copy-start.2 = (bf16[2048,128]{1,0:T(8,128)(2,1)S(1)}, bf16[2048,128]{1,0:T(8,128)(2,1)}, u32[]{:S(2)}) copy-start(bf16[2048,128]{1,0:T(8,128)(2,1)} %param.48) | copy-start | bytes 1572868
  63.1 34.4 %copy-start.7 = (f32[2048]{0:T(1024)S(1)}, f32[2048]{0:T(1024)}, u32[]{:S(2)}) copy-start(f32[2048]{0:T(1024)} %param.41) | copy-start | bytes 24580
  63.8 9.2 %all-to-all-start.3 = ((bf16[4,16,512]{2,0,1:T(4,128)(2,1)}), bf16[4,16,512]{2,0,1:T(4,128)(2,1)S(1)}, u32[]{:S(2)}, u32[]{:S(2)}) async-start(bf16[4,16,512]{2,0,1:T(4,128)(2,1)} %copy.68), calls=%async_computation.3 | async-start | bytes 131072 | tf_op jit(solution)/shard_map/all_to_all | solution.py:137
  67.2 28.8 %all-gather.4.cloned.1.call-start = ((), (), s32[]{:S(2)}) async-start(), calls=%async_computation.6 | async-start | bytes 1179648 | tf_op jit(solution)/shard_map/all_gather | solution.py:71
  74.4 28.0 %copy-start.6 = (bf16[2048,64]{0,1:T(8,128)(2,1)S(1)}, bf16[2048,64]{0,1:T(8,128)(2,1)}, u32[]{:S(2)}) copy-start(bf16[2048,64]{0,1:T(8,128)(2,1)} %param.45) | copy-start | bytes 786436
  98.7 8.7 %all-to-all-start.4 = ((bf16[4,1,8,2048]{3,2,1,0:T(8,128)(2,1)}), bf16[4,1,8,2048]{3,2,1,0:T(8,128)(2,1)S(1)}, u32[]{:S(2)}, u32[]{:S(2)}) async-start(bf16[4,1,8,2048]{3,2,1,0:T(8,128)(2,1)} %fusion.2), calls=%async_computation.4 | async-start | bytes 262144 | tf_op jit(solution)/shard_map/all_to_all | solution.py:185
  112.6 10.2 %copy-start.4 = (bf16[128,2048]{1,0:T(8,128)(2,1)S(1)}, bf16[128,2048]{1,0:T(8,128)(2,1)}, u32[]{:S(2)}) copy-start(bf16[128,2048]{1,0:T(8,128)(2,1)} %param.50) | copy-start | bytes 1572868
  112.6 8.4 %all-to-all-start.5 = ((bf16[4,1,8,2048]{3,2,1,0:T(8,128)(2,1)}), bf16[4,1,8,2048]{3,2,1,0:T(8,128)(2,1)S(1)}, u32[]{:S(2)}, u32[]{:S(2)}) async-start(bf16[4,1,8,2048]{3,2,1,0:T(8,128)(2,1)} %fusion.3), calls=%async_computation.5 | async-start | bytes 262144 | tf_op jit(solution)/shard_map/all_to_all | solution.py:194
  116.0 62.2 %all-reduce.3.cloned.1.call-start = ((), (), s32[]{:S(2)}) async-start(), calls=%async_computation.7 | async-start | bytes 262144
Sparse Core Ops, SparseCore 0:
  75.3 20.7 all-gather.3
  125.1 53.1 all-reduce.2
